TPU v7x, 32 devices: a whole 2x2x4 slice. The times are simulated.
32 devices in a mesh: kv: 4 (over y, x), tp: 8 (over z, core).
Axes of the slice: x: 2, y: 2, z: 4, core: 2. Of those that a mesh axis runs over, the one named last changes fastest.
Arguments:
- tokens: bfloat16 [64, 4096], P(None, ('kv', 'tp')), may hold values from -6 to 6
- memory: float32 [64, 16, 256, 128], P('kv', 'tp'), may hold values from -6 to 6
- normalizer: float32 [64, 16, 128], P('kv', 'tp'), may hold values from -6 to 6
- stabilizer: float32 [64, 16], P('kv', 'tp'), may hold values from -4 to 4
- first_gain: float32 [4096], replicated, may hold values from 0.1 to 1.9
- first_gate: bfloat16 [4096, 12288], P('kv', 'tp'), may hold values from -0.09375 to 0.09375
- first_up: bfloat16 [4096, 12288], P('kv', 'tp'), may hold values from -0.09375 to 0.09375
- first_down: bfloat16 [12288, 4096], P('tp', 'kv'), may hold values from -0.078125 to 0.078125
- mixer_gain: float32 [4096], replicated, may hold values from 0.1 to 1.9
- query_weight: bfloat16 [4096, 2048], P(None, 'tp'), may hold values from -0.09375 to 0.09375
- key_weight: bfloat16 [4096, 2048], P(None, 'tp'), may hold values from -0.09375 to 0.09375
- value_weight: bfloat16 [4096, 4096], P(None, 'tp'), may hold values from -0.09375 to 0.09375
- input_weight: bfloat16 [4096, 16], replicated, may hold values from -0.09375 to 0.09375
- forget_weight: bfloat16 [4096, 16], replicated, may hold values from -0.09375 to 0.09375
- forget_bias: float32 [16], P('tp'), may hold values from -2 to 4
- output_weight: bfloat16 [4096, 4096], P('tp'), may hold values from -0.09375 to 0.09375
- last_gain: float32 [4096], replicated, may hold values from 0.1 to 1.9
- last_gate: bfloat16 [4096, 12288], P('kv', 'tp'), may hold values from -0.09375 to 0.09375
- last_up: bfloat16 [4096, 12288], P('kv', 'tp'), may hold values from -0.09375 to 0.09375
- last_down: bfloat16 [12288, 4096], P('tp', 'kv'), may hold values from -0.078125 to 0.078125
Outputs:
- result: bfloat16 [64, 4096], P(None, ('kv', 'tp'))
- new_memory: float32 [64, 16, 256, 128], P('kv', 'tp')
- new_normalizer: float32 [64, 16, 128], P('kv', 'tp')
- new_stabilizer: float32 [64, 16], P('kv', 'tp')
All inputs are finite; a program needn't handle non-finite values.
Results may differ from a plain program's by a relative error of at most 0.025.
Values may be sent and summed in bfloat16 or wider, within the bound.
A program may use at most 128 MiB of HBM per device.

v0:
```python
import jax
import jax.numpy as jnp
from jax import lax
from jax.sharding import PartitionSpec as P

EPS = 1e-06


def hidden_units(gate_acc, up_acc, squares, model_width):
    scale = lax.rsqrt(squares / model_width + EPS)[:, None]
    return (jax.nn.silu(scale * gate_acc) * (scale * up_acc)).astype(jnp.bfloat16)


def gated_block(block, gain, w_gate, w_up, w_down, model_width):
    f32 = jnp.float32
    width = block.shape[1]
    gain_block = lax.dynamic_slice_in_dim(gain, lax.axis_index("kv") * width, width, 0)
    values = block.astype(f32)
    scaled = (values * gain_block).astype(jnp.bfloat16)
    gate_part = jnp.dot(scaled, w_gate, preferred_element_type=f32)
    up_part = jnp.dot(scaled, w_up, preferred_element_type=f32)
    squares = jnp.sum(values * values, axis=1)
    gate_acc, up_acc, sq_total = (
        lax.psum(gate_part.astype(jnp.bfloat16), "kv").astype(jnp.float32),
        lax.psum(up_part.astype(jnp.bfloat16), "kv").astype(jnp.float32),
        lax.psum(squares.astype(jnp.bfloat16), "kv").astype(jnp.float32),
    )
    hidden = hidden_units(gate_acc, up_acc, sq_total, model_width)
    share = lax.psum_scatter(
        lax.dot_general(
            w_down, hidden, (((0,), (1,)), ((), ())), preferred_element_type=f32
        ).astype(jnp.bfloat16),
        "tp",
        scatter_dimension=0,
        tiled=True,
    ).astype(jnp.float32)
    return share.T


def body(
    tokens,
    memory,
    normalizer,
    stabilizer,
    first_gain,
    first_gate,
    first_up,
    first_down,
    mixer_gain,
    query_weight,
    key_weight,
    value_weight,
    input_weight,
    forget_weight,
    forget_bias,
    output_weight,
    last_gain,
    last_gate,
    last_up,
    last_down,
):
    f32 = jnp.float32
    model_width = first_gain.shape[0]
    rows, col_width = tokens.shape
    block = lax.all_gather(tokens, "tp", axis=1, tiled=True)
    first_share = gated_block(block, first_gain, first_gate, first_up, first_down, model_width)
    stream_one = (tokens.astype(f32) + 0.5 * first_share).astype(jnp.bfloat16)
    seq_count, head_count, value_size, key_size = memory.shape
    moved = lax.all_to_all(
        stream_one.reshape(rows, 1, col_width), "kv", split_axis=0, concat_axis=1, tiled=True
    )
    own_rows = lax.all_gather(moved, "tp", axis=2, tiled=True).reshape(seq_count, model_width)
    row_values = own_rows.astype(f32)
    scale = lax.rsqrt(jnp.mean(row_values * row_values, axis=1, keepdims=True) + EPS)
    cell_in = (row_values * mixer_gain).astype(jnp.bfloat16)
    query = (
        scale * jnp.dot(cell_in, query_weight, preferred_element_type=f32) * key_size ** (-0.5)
    ).reshape(seq_count, head_count, key_size)
    key = (scale * jnp.dot(cell_in, key_weight, preferred_element_type=f32)).reshape(
        seq_count, head_count, key_size
    )
    value = (scale * jnp.dot(cell_in, value_weight, preferred_element_type=f32)).reshape(
        seq_count, head_count, value_size
    )
    first_head = lax.axis_index("tp") * head_count
    input_all = scale * jnp.dot(cell_in, input_weight, preferred_element_type=f32)
    forget_all = scale * jnp.dot(cell_in, forget_weight, preferred_element_type=f32)
    input_pre = lax.dynamic_slice_in_dim(input_all, first_head, head_count, 1)
    log_forget = jax.nn.log_sigmoid(
        lax.dynamic_slice_in_dim(forget_all, first_head, head_count, 1) + forget_bias
    )
    carried = log_forget + stabilizer
    new_stabilizer = jnp.maximum(carried, input_pre)
    keep = jnp.exp(carried - new_stabilizer)
    admit = jnp.exp(input_pre - new_stabilizer)
    recalled = jnp.einsum("bhvd,bhd->bhv", memory, query, precision=lax.Precision.HIGHEST)
    match = jnp.sum(query * key, axis=-1)
    numer = keep[..., None] * recalled + (admit * match)[..., None] * value
    denom = keep * jnp.sum(normalizer * query, axis=-1) + admit * match
    cell_out = (
        (numer / jnp.maximum(jnp.abs(denom), 1.0)[..., None])
        .reshape(seq_count, head_count * value_size)
        .astype(jnp.bfloat16)
    )
    new_memory = (
        keep[..., None, None] * memory
        + admit[..., None, None] * value[..., :, None] * key[..., None, :]
    )
    new_normalizer = keep[..., None] * normalizer + admit[..., None] * key
    partial_heads = jnp.dot(cell_out, output_weight, preferred_element_type=f32)
    mixed = lax.psum(partial_heads.astype(jnp.bfloat16), "tp").astype(jnp.float32)
    rows_two = (row_values + mixed).astype(jnp.bfloat16)
    whole_two = lax.all_to_all(rows_two, "kv", split_axis=1, concat_axis=0, tiled=True)
    last_share = gated_block(whole_two, last_gain, last_gate, last_up, last_down, model_width)
    own_columns = lax.dynamic_slice_in_dim(
        whole_two, lax.axis_index("tp") * col_width, col_width, 1
    )
    result = (own_columns.astype(f32) + 0.5 * last_share).astype(jnp.bfloat16)
    return (result, new_memory, new_normalizer, new_stabilizer)


def solution(mesh):
    in_specs = (
        P(None, ("kv", "tp")),
        P("kv", "tp", None, None),
        P("kv", "tp", None),
        P("kv", "tp"),
        P(),
        P("kv", "tp"),
        P("kv", "tp"),
        P("tp", "kv"),
        P(),
        P(None, "tp"),
        P(None, "tp"),
        P(None, "tp"),
        P(),
        P(),
        P("tp"),
        P("tp", None),
        P(),
        P("kv", "tp"),
        P("kv", "tp"),
        P("tp", "kv"),
    )
    out_specs = (
        P(None, ("kv", "tp")),
        P("kv", "tp", None, None),
        P("kv", "tp", None),
        P("kv", "tp"),
    )
    return jax.shard_map(body, mesh=mesh, in_specs=in_specs, out_specs=out_specs, check_vma=False)
```

profile of v0, /device:TPU:0, one launch (start us, length us, event | category | flops | bytes accessed | tf_op | source)
XLA Modules:
  0.0 307.5 jit_solution(12249599025583255382)
XLA Ops:
  7.2 0.0 all-reduce.10.cloned.1.call-start
  7.2 14.9 %all_gather.6 = bf16[64,1024]{1,0:T(8,128)(2,1)S(1)} all-gather(bf16[64,128]{1,0:T(8,128)(2,1)} %param.20), channel_id=1, replica_groups=mesh['kv'=4,'tp'=8] {'tp'}, dimensions={1}, use_global_device_ids=true | all-gather | bytes 147456 | tf_op jit(solution)/shard_map/all_gather | solution.py:65
  22.1 0.8 dynamic_slice.15
  23.0 1.3 convolution_convert_fusion.3
  24.3 1.3 convolution_convert_fusion.4
  25.6 0.0 all-reduce.10.cloned.1.call-update
  25.6 0.0 reduce-scatter.7.cloned.1.call-start
  25.7 0.1 fusion.3
  25.8 10.0 %psum.49 = bf16[64]{0:T(256)(128)(2,1)S(1)} all-reduce(bf16[64]{0:T(256)(128)(2,1)S(1)} %fusion.3), channel_id=1, replica_groups=mesh['kv'=4,'tp'=8] {'kv'}, use_global_device_ids=true, to_apply=%region_1.0 | all-reduce | flops 64 | bytes 256 | tf_op jit(solution)/shard_map/psum | solution.py:26
  35.8 34.0 %all-reduce.10.cloned.1.call-done = (bf16[64,1536]{1,0:T(8,128)(2,1)}, bf16[64,1536]{1,0:T(8,128)(2,1)}) async-done(((bf16[64,1536]{1,0:T(8,128)(2,1)}, bf16[64,1536]{1,0:T(8,128)(2,1)}), (bf16[64,1536]{1,0:T(8,128)(2,1)}, bf16[64,1536]{1,0:T(8,128)(2,1)})) %all-reduce.10.cloned.1.call-update) | async-done | bytes 393232 | tf_op jit(solution)/shard_map/psum | solution.py:25
  69.8 2.8 fusion
  72.6 0.8 copy.87
  73.5 30.9 %reduce-scatter.7.cloned.1.call-done = bf16[128,64]{1,0:T(8,128)(2,1)} async-done(((bf16[1024,64]{1,0:T(8,128)(2,1)}), bf16[128,64]{1,0:T(8,128)(2,1)}) %reduce-scatter.7.cloned.1.call-update) | async-done | bytes 16400
  104.4 0.8 copy.88
  105.3 0.5 broadcast.65
  105.8 0.7 reduce.3
  106.5 0.6 reshape.77
  107.1 3.7 %all-to-all-start = ((bf16[4,2,1024]{2,1,0:T(2,128)(2,1)}), bf16[4,2,1024]{2,1,0:T(2,128)(2,1)S(1)}, u32[]{:S(2)}, u32[]{:S(2)}) async-start(bf16[4,2,1024]{2,1,0:T(2,128)(2,1)} %reshape.77), calls=%async_computation | async-start | bytes 32768 | tf_op jit(solution)/shard_map/all_to_all | solution.py:69
  110.8 4.7 %all-to-all-done = bf16[4,2,1024]{2,1,0:T(2,128)(2,1)S(1)} async-done(((bf16[4,2,1024]{2,1,0:T(2,128)(2,1)}), bf16[4,2,1024]{2,1,0:T(2,128)(2,1)S(1)}, u32[]{:S(2)}, u32[]{:S(2)}) %all-to-all-start) | async-done | bytes 16416 | tf_op jit(solution)/shard_map/all_to_all | solution.py:69
  115.5 12.8 %all-gather = bf16[16,4,1,1024]{3,0,1,2:T(8,128)(2,1)S(1)} all-gather(bf16[16,4,1,128]{3,0,1,2:T(8,128)(2,1)S(1)} %bitcast.73), channel_id=2, replica_groups=mesh['kv'=4,'tp'=8] {'tp'}, dimensions={3}, use_global_device_ids=true | all-gather | bytes 147456 | tf_op jit(solution)/shard_map/all_gather | solution.py:72
  128.4 0.1 copy.72
  128.5 0.1 multiply_reduce_fusion
  128.6 0.2 copy.94
  128.8 0.5 copy-done.8
  129.4 1.9 fusion.2
  131.3 0.7 reshape.61
  132.0 0.6 reshape.70
  132.6 3.5 %convolution_multiply_fusion = f32[16,512]{1,0:T(8,128)} fusion(bf16[16,4096]{1,0:T(8,128)(2,1)S(1)} %multiply_convert_fusion.3, bf16[4096,512]{1,0:T(8,128)(2,1)} %param.31, f32[16]{0:T(128)} %copy-done.8), kind=kOutput, calls=%fused_computation.10 | convolution fusion | flops 67117056 | bytes 4358208 | tf_op jit(solution)/shard_map/dot_general | solution.py:82
  136.0 1.4 reshape.63
  137.4 2.6 convolution_multiply_fusion.1
  140.0 0.7 reshape.62
  140.7 1.4 multiply_reduce_fusion.2
  142.2 1.3 copy.76
  143.5 1.3 copy.74
  144.8 1.1 fusion.26
  145.9 1.1 fusion.25
  147.0 1.4 abs_maximum_fusion
  148.4 0.1 copy.82
  148.5 0.1 copy.77
  148.5 0.1 copy.75
  148.6 0.1 copy.73
  148.7 5.8 %fusion.27 = f32[16,2,1,256]{3,2,1,0:T(1,128)S(1)} fusion(f32[16,2,128,1]{2,3,1,0:T(1,128)} %bitcast.71, f32[16,2,256,128]{3,2,1,0:T(8,128)} %param.21), kind=kOutput, calls=%fused_computation.61 | convolution fusion | flops 12582912 | bytes 4243456 | tf_op jit(solution)/shard_map/bhvd,bhd->bhv/dot_general | solution.py:96
  154.5 0.1 broadcast_multiply_fusion
  154.7 1.3 convolution_convert_fusion
  156.1 51.8 %all-reduce.6.cloned.1.call-done = bf16[16,4096]{1,0:T(8,128)(2,1)} async-done(((bf16[16,4096]{1,0:T(8,128)(2,1)}), bf16[16,4096]{1,0:T(8,128)(2,1)}) %all-reduce.6.cloned.1.call-update) | async-done | bytes 131088 | tf_op jit(solution)/shard_map/psum | solution.py:111
  207.9 0.9 add_convert_fusion
  208.8 0.7 copy.100
  209.5 3.6 %all-to-all-start.1 = ((bf16[16,4,1024]{2,0,1:T(8,128)(2,1)}), bf16[16,4,1024]{2,0,1:T(8,128)(2,1)S(1)}, u32[]{:S(2)}, u32[]{:S(2)}) async-start(bf16[16,4,1024]{2,0,1:T(8,128)(2,1)} %bitcast.63), calls=%async_computation.1 | async-start | bytes 262144 | tf_op jit(solution)/shard_map/all_to_all | solution.py:113
  213.1 0.7 dynamic_slice.19
  213.8 4.3 %all-to-all-done.1 = bf16[16,4,1024]{2,0,1:T(8,128)(2,1)S(1)} async-done(((bf16[16,4,1024]{2,0,1:T(8,128)(2,1)}), bf16[16,4,1024]{2,0,1:T(8,128)(2,1)S(1)}, u32[]{:S(2)}, u32[]{:S(2)}) %all-to-all-start.1) | async-done | bytes 131104 | tf_op jit(solution)/shard_map/all_to_all | solution.py:113
  218.2 3.4 %convolution_convert_fusion.1 = bf16[64,1536]{1,0:T(8,128)(2,1)} fusion(bf16[1024,1536]{1,0:T(8,128)(2,1)} %param.38, bf16[64,1024]{1,0:T(8,128)(2,1)S(1)} %bitcast.66, f32[1024]{0:T(1024)S(1)} %dynamic_slice.19), kind=kOutput, calls=%fused_computation.2 | convolution fusion | flops 201621504 | bytes 3477504 | tf_op jit(solution)/shard_map/dot_general | solution.py:21
  221.5 1.3 convolution_convert_fusion.2
  222.9 0.0 reduce-scatter.9.cloned.1.call-start
  222.9 0.1 multiply_reduce_fusion.1
  223.0 0.1 convert_element_type.143
  223.1 8.5 %psum.53 = bf16[64]{0:T(256)(128)(2,1)S(1)} all-reduce(bf16[64]{0:T(256)(128)(2,1)S(1)} %convert_element_type.143), channel_id=1, replica_groups=mesh['kv'=4,'tp'=8] {'kv'}, use_global_device_ids=true, to_apply=%region_10.11 | all-reduce | flops 64 | bytes 256 | tf_op jit(solution)/shard_map/psum | solution.py:26
  231.6 33.2 %all-reduce.8.cloned.1.call-done = (bf16[64,1536]{1,0:T(8,128)(2,1)}, bf16[64,1536]{1,0:T(8,128)(2,1)}) async-done(((bf16[64,1536]{1,0:T(8,128)(2,1)}, bf16[64,1536]{1,0:T(8,128)(2,1)}), (bf16[64,1536]{1,0:T(8,128)(2,1)}, bf16[64,1536]{1,0:T(8,128)(2,1)})) %all-reduce.8.cloned.1.call-update) | async-done | bytes 393232 | tf_op jit(solution)/shard_map/psum | solution.py:25
  264.8 2.8 fusion.1
  267.6 0.8 copy.89
  268.5 4.2 %multiply_add_fusion = f32[16,2,256,128]{3,2,1,0:T(8,128)} fusion(f32[16,2,256,128]{3,2,1,0:T(8,128)} %param.21, f32[16,2,128]{2,1,0:T(2,128)S(1)} %reshape.62, f32[16,2,256]{2,1,0:T(2,128)S(1)} %get-tuple-element.15, f32[16,2]{1,0:T(8,128)S(1)} %copy.73), kind=kLoop, calls=%fused_computation.1 | loop fusion | flops 3145728 | bytes 8437888 | tf_op jit(solution)/shard_map/add | solution.py:106
  272.7 0.7 multiply_add_fusion.1
  273.5 26.0 %reduce-scatter.9.cloned.1.call-done = bf16[128,64]{1,0:T(8,128)(2,1)} async-done(((bf16[1024,64]{1,0:T(8,128)(2,1)}), bf16[128,64]{1,0:T(8,128)(2,1)}) %reduce-scatter.9.cloned.1.call-update) | async-done | bytes 16400
  299.5 0.8 copy.90
  300.3 0.6 fusion.11
  (33 shorter events, 0.2 us)
Async XLA Ops:
  7.2 15.8 %copy-start = (bf16[1024,1536]{1,0:T(8,128)(2,1)S(1)}, bf16[1024,1536]{1,0:T(8,128)(2,1)}, u32[]{:S(2)}) copy-start(bf16[1024,1536]{1,0:T(8,128)(2,1)} %param.26) | copy-start | bytes 9437188
  7.2 62.6 %all-reduce.10.cloned.1.call-start = ((), (), s32[]{:S(2)}) async-start(), calls=%async_computation.8 | async-start | bytes 786432 | tf_op jit(solution)/shard_map/psum | solution.py:25
  22.1 2.2 copy-start.2
  25.6 79.7 %copy-start.5 = (bf16[64,128]{1,0:T(8,128)(2,1)S(1)}, bf16[64,128]{1,0:T(8,128)(2,1)}, u32[]{:S(2)}) copy-start(bf16[64,128]{1,0:T(8,128)(2,1)} %param.20) | copy-start | bytes 49156
  25.6 78.8 %reduce-scatter.7.cloned.1.call-start = ((), (), s32[]{:S(2)}) async-start(), calls=%async_computation.5 | async-start | bytes 294912
  69.8 59.0 %copy-start.7 = (f32[4096]{0:T(1024)S(1)}, f32[4096]{0:T(1024)}, u32[]{:S(2)}) copy-start(f32[4096]{0:T(1024)} %param.28) | copy-start | bytes 49156
  107.1 8.4 %all-to-all-start = ((bf16[4,2,1024]{2,1,0:T(2,128)(2,1)}), bf16[4,2,1024]{2,1,0:T(2,128)(2,1)S(1)}, u32[]{:S(2)}, u32[]{:S(2)}) async-start(bf16[4,2,1024]{2,1,0:T(2,128)(2,1)} %reshape.77), calls=%async_computation | async-start | bytes 32768 | tf_op jit(solution)/shard_map/all_to_all | solution.py:69
  110.8 97.1 %all-reduce.6.cloned.1.call-start = ((), (), s32[]{:S(2)}) async-start(), calls=%async_computation.4 | async-start | bytes 262144 | tf_op jit(solution)/shard_map/psum | solution.py:111
  128.8 0.6 copy-start.8
  132.6 4.8 %copy-start.9 = (f32[16]{0:T(128)S(1)}, f32[16]{0:T(128)}, u32[]{:S(2)}) copy-start(f32[16]{0:T(128)} %copy-done.8) | copy-start | bytes 196
  147.0 7.6 %copy-start.4 = (f32[16,2,256]{2,1,0:T(2,128)S(1)}, f32[16,2,256]{2,1,0:T(2,128)}, u32[]{:S(2)}) copy-start(f32[16,2,256]{2,1,0:T(2,128)} %reshape.63) | copy-start | bytes 98308
  148.7 6.0 %copy-start.1 = (bf16[512,4096]{1,0:T(8,128)(2,1)S(1)}, bf16[512,4096]{1,0:T(8,128)(2,1)}, u32[]{:S(2)}) copy-start(bf16[512,4096]{1,0:T(8,128)(2,1)} %param.35) | copy-start | bytes 12582916
  209.5 8.7 %all-to-all-start.1 = ((bf16[16,4,1024]{2,0,1:T(8,128)(2,1)}), bf16[16,4,1024]{2,0,1:T(8,128)(2,1)S(1)}, u32[]{:S(2)}, u32[]{:S(2)}) async-start(bf16[16,4,1024]{2,0,1:T(8,128)(2,1)} %bitcast.63), calls=%async_computation.1 | async-start | bytes 262144 | tf_op jit(solution)/shard_map/all_to_all | solution.py:113
  213.1 51.7 %all-reduce.8.cloned.1.call-start = ((), (), s32[]{:S(2)}) async-start(), calls=%async_computation.7 | async-start | bytes 786432 | tf_op jit(solution)/shard_map/psum | solution.py:25
  218.2 3.4 %copy-start.3 = (bf16[1024,1536]{1,0:T(8,128)(2,1)S(1)}, bf16[1024,1536]{1,0:T(8,128)(2,1)}, u32[]{:S(2)}) copy-start(bf16[1024,1536]{1,0:T(8,128)(2,1)} %param.37) | copy-start | bytes 9437188
  222.9 76.6 %reduce-scatter.9.cloned.1.call-start = ((), (), s32[]{:S(2)}) async-start(), calls=%async_computation.6 | async-start | bytes 294912
  268.5 4.2 %copy-start.6 = (f32[16,2,128]{2,1,0:T(2,128)S(1)}, f32[16,2,128]{2,1,0:T(2,128)}, u32[]{:S(2)}) copy-start(f32[16,2,128]{2,1,0:T(2,128)} %param.22) | copy-start | bytes 49156
Sparse Core Ops, SparseCore 0:
  25.7 44.0 all-reduce.9
  73.6 30.7 reduce-scatter.6
  156.2 51.6 all-reduce.5
  223.0 41.7 all-reduce.7
  268.6 30.7 reduce-scatter.8
where the time goes:
time: 308 us; the launch traced here: 307 us
  waiting for transfers between devices  185 us (60%)
  blocking collectives  46.2 us (15%)
  matrix products  30.2 us (10%)
  local copies, waits for them, and re-layouts  14 us (5%)
  between operations  13.9 us (5%)
  other arithmetic  10.6 us (3%)
  starting transfers between devices  7.45 us (2%)
    psum x2, waiting for transfers between devices, gated_block(): lax.psum(up_part.astype(jnp.bfloat16), 'kv').astype(jnp.float32)  67.2 us
    unnamed x7, waiting for transfers between devices  57 us
    psum x1, waiting for transfers between devices, body(): lax.psum(partial_heads.astype(jnp.bfloat16), 'tp').astype(jnp.float32)  51.8 us
    psum x2, blocking collectives, gated_block(): lax.psum(squares.astype(jnp.bfloat16), 'kv').astype(jnp.float32)  18.5 us
    all_gather x1, blocking collectives, body(): block = lax.all_gather(tokens, 'tp', axis=1, tiled=True)  14.9 us
    all_gather x1, blocking collectives, body(): lax.all_gather(moved, 'tp', axis=2, tiled=True)  12.8 us
  transfers between devices with their start and end apart: 7, of which 7 were waited for; matrix products, arithmetic and copies ran while one was open for 2% of the time, Pallas kernels for 0%

commit v1 on v0

--- a/solution.py
+++ b/solution.py
@@ -108,7 +108,9 @@
     )
     new_normalizer = keep[..., None] * normalizer + admit[..., None] * key
     partial_heads = jnp.dot(cell_out, output_weight, preferred_element_type=f32)
-    mixed = lax.psum(partial_heads.astype(jnp.bfloat16), "tp").astype(jnp.float32)
+    mixed = jnp.sum(lax.all_gather(partial_heads.astype(jnp.bfloat16), "tp"), axis=0).astype(
+        jnp.float32
+    )
     rows_two = (row_values + mixed).astype(jnp.bfloat16)
     whole_two = lax.all_to_all(rows_two, "kv", split_axis=1, concat_axis=0, tiled=True)
     last_share = gated_block(whole_two, last_gain, last_gate, last_up, last_down, model_width)

time: 308 us -> 267 us (0.87)
  waiting for transfers between devices: 185 us -> 153 us
  local copies, waits for them, and re-layouts: 14 us -> 7.1 us
    psum x1 -> x0, waiting for transfers between devices: 51.8 us -> none  [body(): lax.psum(partial_heads.astype(jnp.bfloat16), 'tp').astype(jnp.float32)]
    all_gather x0 -> x1, waiting for transfers between devices: none -> 19.1 us  [body(): lax.all_gather(partial_heads.astype(jnp.bfloat16), 'tp')]
where the time goes in v1:
time: 267 us; the launch traced here: 266 us
  waiting for transfers between devices  153 us (57%)
  blocking collectives  46.2 us (17%)
  matrix products  28.9 us (11%)
  between operations  14 us (5%)
  other arithmetic  9.67 us (4%)
  starting transfers between devices  7.45 us (3%)
  local copies, waits for them, and re-layouts  7.1 us (3%)
    psum x2, waiting for transfers between devices, gated_block(): lax.psum(up_part.astype(jnp.bfloat16), 'kv').astype(jnp.float32)  67.7 us
    unnamed x7, waiting for transfers between devices  57 us
    all_gather x1, waiting for transfers between devices, body(): lax.all_gather(partial_heads.astype(jnp.bfloat16), 'tp')  19.1 us
    psum x2, blocking collectives, gated_block(): lax.psum(squares.astype(jnp.bfloat16), 'kv').astype(jnp.float32)  18.5 us
    all_gather x1, blocking collectives, body(): block = lax.all_gather(tokens, 'tp', axis=1, tiled=True)  14.9 us
    all_gather x1, blocking collectives, body(): lax.all_gather(moved, 'tp', axis=2, tiled=True)  12.8 us
    dot_general x1, matrix products, body(): jnp.einsum('bhvd,bhd->bhv', memory, query, precision=lax.Precision.HIGHEST)  5.81 us
    dot_general x2, matrix products, gated_block(): lax.dot_general(w_down, hidden, (((0,), (1,)), ((), ())), preferred_eleme...  5.66 us
  transfers between devices with their start and end apart: 7, of which 7 were waited for; matrix products, arithmetic and copies ran while one was open for 2% of the time, Pallas kernels for 0%

profile of v1, /device:TPU:0, one launch (start us, length us, event | category | flops | bytes accessed | tf_op | source)
XLA Modules:
  0.0 266.2 jit_solution(9406851130459628984)
XLA Ops:
  7.2 0.0 all-reduce.7.cloned.1.call-start
  7.2 14.9 %all_gather.12 = bf16[64,1024]{1,0:T(8,128)(2,1)S(1)} all-gather(bf16[64,128]{1,0:T(8,128)(2,1)} %param.20), channel_id=1, replica_groups=mesh['kv'=4,'tp'=8] {'tp'}, dimensions={1}, use_global_device_ids=true | all-gather | bytes 147456 | tf_op jit(solution)/shard_map/all_gather | solution.py:65
  22.1 0.8 dynamic_slice.15
  23.0 1.3 convolution_convert_fusion.3
  24.3 1.3 convolution_convert_fusion.4
  25.6 0.0 all-reduce.7.cloned.1.call-update
  25.6 0.0 reduce-scatter.7.cloned.1.call-start
  25.7 0.1 fusion.3
  25.8 10.0 %psum.42 = bf16[64]{0:T(256)(128)(2,1)S(1)} all-reduce(bf16[64]{0:T(256)(128)(2,1)S(1)} %fusion.3), channel_id=1, replica_groups=mesh['kv'=4,'tp'=8] {'kv'}, use_global_device_ids=true, to_apply=%region_1.0 | all-reduce | flops 64 | bytes 256 | tf_op jit(solution)/shard_map/psum | solution.py:26
  35.8 34.0 %all-reduce.7.cloned.1.call-done = (bf16[64,1536]{1,0:T(8,128)(2,1)}, bf16[64,1536]{1,0:T(8,128)(2,1)}) async-done(((bf16[64,1536]{1,0:T(8,128)(2,1)}, bf16[64,1536]{1,0:T(8,128)(2,1)}), (bf16[64,1536]{1,0:T(8,128)(2,1)}, bf16[64,1536]{1,0:T(8,128)(2,1)})) %all-reduce.7.cloned.1.call-update) | async-done | bytes 393232 | tf_op jit(solution)/shard_map/psum | solution.py:25
  69.8 2.8 %fusion = bf16[1024,64]{0,1:T(8,128)(2,1)S(1)} fusion(bf16[1536,1024]{1,0:T(8,128)(2,1)} %param.27, bf16[64,1536]{1,0:T(8,128)(2,1)} %get-tuple-element.8, bf16[64,1536]{1,0:T(8,128)(2,1)} %get-tuple-element.9, f32[64]{0:T(128)S(1)} %add_rsqrt_fusion.2), kind=kOutput, calls=%fused_computation.8 | convolution fusion | flops 202375168 | bytes 3670272 | tf_op jit(solution)/shard_map/dot_general | solution.py:30
  72.6 0.8 copy.83
  73.5 0.0 reduce-scatter.7.cloned.1.call-update
  73.5 30.9 %reduce-scatter.7.cloned.1.call-done = bf16[128,64]{1,0:T(8,128)(2,1)} async-done(((bf16[1024,64]{1,0:T(8,128)(2,1)}), bf16[128,64]{1,0:T(8,128)(2,1)}) %reduce-scatter.7.cloned.1.call-update) | async-done | bytes 16400
  104.4 0.8 copy.84
  105.3 0.5 broadcast.65
  105.8 0.7 reduce.3
  106.5 0.6 reshape.81
  107.1 3.7 %all-to-all-start = ((bf16[4,2,1024]{2,1,0:T(2,128)(2,1)}), bf16[4,2,1024]{2,1,0:T(2,128)(2,1)S(1)}, u32[]{:S(2)}, u32[]{:S(2)}) async-start(bf16[4,2,1024]{2,1,0:T(2,128)(2,1)} %reshape.81), calls=%async_computation | async-start | bytes 32768 | tf_op jit(solution)/shard_map/all_to_all | solution.py:69
  110.8 4.7 %all-to-all-done = bf16[4,2,1024]{2,1,0:T(2,128)(2,1)S(1)} async-done(((bf16[4,2,1024]{2,1,0:T(2,128)(2,1)}), bf16[4,2,1024]{2,1,0:T(2,128)(2,1)S(1)}, u32[]{:S(2)}, u32[]{:S(2)}) %all-to-all-start) | async-done | bytes 16416 | tf_op jit(solution)/shard_map/all_to_all | solution.py:69
  115.5 12.8 %all-gather = bf16[16,4,1,1024]{3,0,1,2:T(8,128)(2,1)S(1)} all-gather(bf16[16,4,1,128]{3,0,1,2:T(8,128)(2,1)S(1)} %bitcast.80), channel_id=2, replica_groups=mesh['kv'=4,'tp'=8] {'tp'}, dimensions={3}, use_global_device_ids=true | all-gather | bytes 147456 | tf_op jit(solution)/shard_map/all_gather | solution.py:72
  128.4 0.1 copy.68
  128.5 0.1 fusion.6
  128.6 0.2 copy.90
  128.8 1.9 fusion.2
  130.8 0.1 reshape.64
  130.9 2.8 %convolution_multiply_fusion = f32[16,512]{1,0:T(8,128)S(1)} fusion(bf16[16,4096]{1,0:T(8,128)(2,1)S(1)} %multiply_convert_fusion.3, bf16[4096,512]{1,0:T(8,128)(2,1)} %param.31, f32[16]{0:T(128)S(1)} %add_rsqrt_fusion.1), kind=kOutput, calls=%fused_computation.10 | convolution fusion | flops 67117056 | bytes 4358208 | tf_op jit(solution)/shard_map/dot_general | solution.py:82
  133.7 0.1 reshape.66
  133.8 1.9 convolution_multiply_fusion.1
  135.7 0.1 reshape.65
  135.8 0.1 multiply_reduce_fusion.1
  135.9 0.1 copy.72
  136.0 0.1 copy.70
  136.0 1.1 fusion.28
  137.1 1.1 fusion.27
  138.2 0.7 abs_maximum_fusion
  138.9 0.1 copy.78
  138.9 0.1 copy.73
  139.0 0.1 copy.71
  139.1 0.1 copy.69
  139.2 5.8 %fusion.29 = f32[16,2,1,256]{3,2,1,0:T(1,128)S(1)} fusion(f32[16,2,128,1]{2,3,1,0:T(1,128)S(1)} %bitcast.78, f32[16,2,256,128]{3,2,1,0:T(8,128)} %param.21), kind=kOutput, calls=%fused_computation.62 | convolution fusion | flops 12582912 | bytes 4243456 | tf_op jit(solution)/shard_map/bhvd,bhd->bhv/dot_general | solution.py:96
  145.0 0.1 broadcast_multiply_fusion
  145.2 1.3 convolution_convert_fusion
  146.5 0.0 all-gather.4.cloned.1.call-update
  146.5 19.1 %all-gather.4.cloned.1.call-done = bf16[128,4096]{1,0:T(8,128)(2,1)} async-done(((bf16[16,4096]{1,0:T(8,128)(2,1)}), bf16[128,4096]{1,0:T(8,128)(2,1)}) %all-gather.4.cloned.1.call-update) | async-done | bytes 1048592 | tf_op jit(solution)/shard_map/all_gather | solution.py:111
  165.6 1.4 reduce_sum.61
  167.0 0.7 fusion.5
  167.7 3.6 %all-to-all-start.1 = ((bf16[16,4,1024]{2,0,1:T(8,128)(2,1)}), bf16[16,4,1024]{2,0,1:T(8,128)(2,1)S(1)}, u32[]{:S(2)}, u32[]{:S(2)}) async-start(bf16[16,4,1024]{2,0,1:T(8,128)(2,1)} %fusion.5), calls=%async_computation.1 | async-start | bytes 262144 | tf_op jit(solution)/shard_map/all_to_all | solution.py:115
  171.3 0.7 dynamic_slice.19
  172.0 4.3 %all-to-all-done.1 = bf16[16,4,1024]{2,0,1:T(8,128)(2,1)S(1)} async-done(((bf16[16,4,1024]{2,0,1:T(8,128)(2,1)}), bf16[16,4,1024]{2,0,1:T(8,128)(2,1)S(1)}, u32[]{:S(2)}, u32[]{:S(2)}) %all-to-all-start.1) | async-done | bytes 131104 | tf_op jit(solution)/shard_map/all_to_all | solution.py:115
  176.4 3.4 %convolution_convert_fusion.1 = bf16[64,1536]{1,0:T(8,128)(2,1)} fusion(bf16[1024,1536]{1,0:T(8,128)(2,1)} %param.38, bf16[64,1024]{1,0:T(8,128)(2,1)S(1)} %bitcast.71, f32[1024]{0:T(1024)S(1)} %dynamic_slice.19), kind=kOutput, calls=%fused_computation.2 | convolution fusion | flops 201621504 | bytes 3477504 | tf_op jit(solution)/shard_map/dot_general | solution.py:21
  179.7 1.3 convolution_convert_fusion.2
  181.1 0.0 reduce-scatter.9.cloned.1.call-start
  181.1 0.1 multiply_reduce_fusion
  181.2 0.1 convert_element_type.152
  181.3 8.5 %psum.45 = bf16[64]{0:T(256)(128)(2,1)S(1)} all-reduce(bf16[64]{0:T(256)(128)(2,1)S(1)} %convert_element_type.152), channel_id=1, replica_groups=mesh['kv'=4,'tp'=8] {'kv'}, use_global_device_ids=true, to_apply=%region_10.11 | all-reduce | flops 64 | bytes 256 | tf_op jit(solution)/shard_map/psum | solution.py:26
  189.8 33.8 %all-reduce.5.cloned.1.call-done = (bf16[64,1536]{1,0:T(8,128)(2,1)}, bf16[64,1536]{1,0:T(8,128)(2,1)}) async-done(((bf16[64,1536]{1,0:T(8,128)(2,1)}, bf16[64,1536]{1,0:T(8,128)(2,1)}), (bf16[64,1536]{1,0:T(8,128)(2,1)}, bf16[64,1536]{1,0:T(8,128)(2,1)})) %all-reduce.5.cloned.1.call-update) | async-done | bytes 393232 | tf_op jit(solution)/shard_map/psum | solution.py:25
  223.6 2.8 %fusion.1 = bf16[1024,64]{0,1:T(8,128)(2,1)S(1)} fusion(bf16[1536,1024]{1,0:T(8,128)(2,1)} %param.39, bf16[64,1536]{1,0:T(8,128)(2,1)} %get-tuple-element.6, bf16[64,1536]{1,0:T(8,128)(2,1)} %get-tuple-element.7, f32[64]{0:T(128)S(1)} %add_rsqrt_fusion), kind=kOutput, calls=%fused_computation.9 | convolution fusion | flops 202375168 | bytes 3670272 | tf_op jit(solution)/shard_map/dot_general | solution.py:30
  226.4 0.8 copy.85
  227.2 4.2 %multiply_add_fusion = f32[16,2,256,128]{3,2,1,0:T(8,128)} fusion(f32[16,2,256,128]{3,2,1,0:T(8,128)} %param.21, f32[16,2,128]{2,1,0:T(2,128)S(1)} %reshape.65, f32[16,2,256]{2,1,0:T(2,128)S(1)} %get-tuple-element.15, f32[16,2]{1,0:T(8,128)S(1)} %copy.69), kind=kLoop, calls=%fused_computation.1 | loop fusion | flops 3145728 | bytes 8437888 | tf_op jit(solution)/shard_map/add | solution.py:106
  231.5 0.7 multiply_add_fusion.1
  232.2 26.0 %reduce-scatter.9.cloned.1.call-done = bf16[128,64]{1,0:T(8,128)(2,1)} async-done(((bf16[1024,64]{1,0:T(8,128)(2,1)}), bf16[128,64]{1,0:T(8,128)(2,1)}) %reduce-scatter.9.cloned.1.call-update) | async-done | bytes 16400
  258.2 0.8 copy.86
  259.0 0.6 fusion.13
  (32 shorter events, 0.2 us)
Async XLA Ops:
  7.2 15.8 %copy-start = (bf16[1024,1536]{1,0:T(8,128)(2,1)S(1)}, bf16[1024,1536]{1,0:T(8,128)(2,1)}, u32[]{:S(2)}) copy-start(bf16[1024,1536]{1,0:T(8,128)(2,1)} %param.26) | copy-start | bytes 9437188
  7.2 62.6 %all-reduce.7.cloned.1.call-start = ((), (), s32[]{:S(2)}) async-start(), calls=%async_computation.8 | async-start | bytes 786432 | tf_op jit(solution)/shard_map/psum | solution.py:25
  22.1 2.2 copy-start.2
  25.6 79.7 %copy-start.4 = (bf16[64,128]{1,0:T(8,128)(2,1)S(1)}, bf16[64,128]{1,0:T(8,128)(2,1)}, u32[]{:S(2)}) copy-start(bf16[64,128]{1,0:T(8,128)(2,1)} %param.20) | copy-start | bytes 49156
  25.6 78.8 %reduce-scatter.7.cloned.1.call-start = ((), (), s32[]{:S(2)}) async-start(), calls=%async_computation.5 | async-start | bytes 294912
  69.8 59.0 %copy-start.6 = (f32[4096]{0:T(1024)S(1)}, f32[4096]{0:T(1024)}, u32[]{:S(2)}) copy-start(f32[4096]{0:T(1024)} %param.28) | copy-start | bytes 49156
  107.1 8.4 %all-to-all-start = ((bf16[4,2,1024]{2,1,0:T(2,128)(2,1)}), bf16[4,2,1024]{2,1,0:T(2,128)(2,1)S(1)}, u32[]{:S(2)}, u32[]{:S(2)}) async-start(bf16[4,2,1024]{2,1,0:T(2,128)(2,1)} %reshape.81), calls=%async_computation | async-start | bytes 32768 | tf_op jit(solution)/shard_map/all_to_all | solution.py:69
  110.8 54.8 %all-gather.4.cloned.1.call-start = ((), (), s32[]{:S(2)}) async-start(), calls=%async_computation.4 | async-start | bytes 1179648 | tf_op jit(solution)/shard_map/all_gather | solution.py:111
  130.8 4.9 %copy-start.5 = (f32[16,2,128]{2,1,0:T(2,128)S(1)}, f32[16,2,128]{2,1,0:T(2,128)}, u32[]{:S(2)}) copy-start(f32[16,2,128]{2,1,0:T(2,128)} %param.22) | copy-start | bytes 49156
  130.9 7.3 %copy-start.7 = (f32[16,2]{0,1:T(2,128)S(1)}, f32[16,2]{0,1:T(2,128)}, u32[]{:S(2)}) copy-start(f32[16,2]{0,1:T(2,128)} %param.23) | copy-start | bytes 388
  130.9 7.3 %copy-start.8 = (f32[2]{0:T(128)S(1)}, f32[2]{0:T(128)}, u32[]{:S(2)}) copy-start(f32[2]{0:T(128)} %param.34) | copy-start | bytes 28
  139.2 6.0 %copy-start.1 = (bf16[512,4096]{1,0:T(8,128)(2,1)S(1)}, bf16[512,4096]{1,0:T(8,128)(2,1)}, u32[]{:S(2)}) copy-start(bf16[512,4096]{1,0:T(8,128)(2,1)} %param.35) | copy-start | bytes 12582916
  167.7 8.7 %all-to-all-start.1 = ((bf16[16,4,1024]{2,0,1:T(8,128)(2,1)}), bf16[16,4,1024]{2,0,1:T(8,128)(2,1)S(1)}, u32[]{:S(2)}, u32[]{:S(2)}) async-start(bf16[16,4,1024]{2,0,1:T(8,128)(2,1)} %fusion.5), calls=%async_computation.1 | async-start | bytes 262144 | tf_op jit(solution)/shard_map/all_to_all | solution.py:115
  171.3 52.2 %all-reduce.5.cloned.1.call-start = ((), (), s32[]{:S(2)}) async-start(), calls=%async_computation.7 | async-start | bytes 786432 | tf_op jit(solution)/shard_map/psum | solution.py:25
  176.4 3.4 %copy-start.3 = (bf16[1024,1536]{1,0:T(8,128)(2,1)S(1)}, bf16[1024,1536]{1,0:T(8,128)(2,1)}, u32[]{:S(2)}) copy-start(bf16[1024,1536]{1,0:T(8,128)(2,1)} %param.37) | copy-start | bytes 9437188
  181.1 77.1 %reduce-scatter.9.cloned.1.call-start = ((), (), s32[]{:S(2)}) async-start(), calls=%async_computation.6 | async-start | bytes 294912
Sparse Core Ops, SparseCore 0:
  25.7 44.0 all-reduce.6
  73.6 30.7 reduce-scatter.6
  146.7 18.8 all-gather.3
  181.2 42.3 all-reduce.4
  227.4 30.7 reduce-scatter.8
